TPU v7x, 32 devices: a whole 2x2x4 slice. The times are simulated.
32 devices in a mesh: kv: 16 (over z, y, core), tp: 2 (over x).
Axes of the slice: x: 2, y: 2, z: 4, core: 2. Of those that a mesh axis runs over, the one named last changes fastest.
Arguments:
- queries: bfloat16 [4096, 1536], P('kv', 'tp'), may hold values from -6 to 6
- keys: bfloat16 [4096, 256], P('kv', 'tp'), may hold values from -6 to 6
- values: bfloat16 [4096, 256], P('kv', 'tp'), may hold values from -6 to 6
- log_sums: float32 [12, 4096], P('tp', 'kv'), may hold values from 6 to 7.5
- out_grad: bfloat16 [4096, 1536], P('kv', 'tp'), may hold values from -6 to 6
- chosen: int32 [64, 2, 8], P('kv', 'tp'), may hold values from 0 to 63, as said below
- inputs: bfloat16 [4096, 3072], P('kv', 'tp'), may hold values from -6 to 6
Outputs:
- query_grad: bfloat16 [4096, 1536], P('kv', 'tp')
- key_grad: bfloat16 [4096, 256], P('kv', 'tp')
- value_grad: bfloat16 [4096, 256], P('kv', 'tp')
- weight_grad: float32 [3072, 256], P('kv', 'tp')
Inputs may be any that keep to these rules, and one draw needn't show every extreme that they name: `chosen`: for query block g and key head h, every slot holds g (an empty slot) or a key block c with g - 16 <= c < g; the blocks of the live slots of one list are distinct; each list has between 4 and 8 live slots, except that query block g has at most g of them (block 0 has none).
All inputs are finite; a program needn't handle non-finite values.
Results may differ from a plain program's by a relative error of at most 0.0049.
Values may be sent and summed in bfloat16 or wider, within the bound.
A program may use at most 64 MiB of HBM per device.

v0:
```python
import jax
import jax.numpy as jnp
from jax import lax
from jax.sharding import PartitionSpec as P

SEL = 8
REACH = 4


def passed_along(value, axis, steps):
    count = lax.axis_size(axis)
    leading, last = (max(0, -steps), min(count, count - steps))
    return lax.ppermute(value, axis, [(source, source + steps) for source in range(leading, last)])


def tile_grads(
    query_tile_set,
    gradient_tiles,
    sum_tiles,
    key_matrix_rows,
    value_matrix_rows,
    permitted_mask,
    scaling,
):
    scores = (
        jnp.einsum(
            "nevu,npu->nvep", query_tile_set, key_matrix_rows, preferred_element_type=jnp.float32
        )
        * scaling
    )
    weights = jnp.where(permitted_mask[:, None], jnp.exp(scores - sum_tiles[..., None]), 0.0)
    grad_weights = jnp.einsum(
        "nevu,npu->nvep", gradient_tiles, value_matrix_rows, preferred_element_type=jnp.float32
    )
    delta_rows = jnp.sum(weights * grad_weights, -1, keepdims=True)
    score_gradient = (weights * (grad_weights - delta_rows)).astype(jnp.bfloat16)
    weights_reduced = weights.astype(jnp.bfloat16)
    query_part = (
        jnp.einsum(
            "nlpv,nvu->nplu", score_gradient, key_matrix_rows, preferred_element_type=jnp.float32
        )
        * scaling
    )
    key_part = (
        jnp.einsum(
            "cxie,cixa->cea", score_gradient, query_tile_set, preferred_element_type=jnp.float32
        )
        * scaling
    )
    value_part = jnp.einsum(
        "cxie,cixa->cea", weights_reduced, gradient_tiles, preferred_element_type=jnp.float32
    )
    return (query_part, key_part, value_part)


def shards(queries, keys, values, log_sums, out_grad, chosen, inputs):
    tok_rows = keys.shape[0]
    blocks_dev = chosen.shape[0]
    block_length = tok_rows // blocks_dev
    head_dim = keys.shape[1]
    group_size = queries.shape[1] // head_dim
    scaling = head_dim ** (-0.5)
    window_blocks = (REACH + 1) * blocks_dev
    device = lax.axis_index("kv")
    earlier = []
    for offset in range(REACH, 0, -1):
        earlier.append(passed_along((keys, values), "kv", offset))
    win_keys = jnp.concatenate([pair[0] for pair in earlier] + [keys], 0)
    win_values = jnp.concatenate([pair[1] for pair in earlier] + [values], 0)
    listed = chosen[:, 0, :]
    global_ids = device * blocks_dev + jnp.arange(blocks_dev, dtype=jnp.int32)
    live_slots = listed < global_ids[:, None]
    local_ids = listed - (device - REACH) * blocks_dev
    own_index = REACH * blocks_dev + jnp.arange(blocks_dev, dtype=jnp.int32)
    query_tile_set = queries.reshape(blocks_dev, block_length, group_size, head_dim)
    gradient_tiles = out_grad.reshape(blocks_dev, block_length, group_size, head_dim)
    sum_tiles = log_sums.reshape(group_size, blocks_dev, block_length).transpose(1, 0, 2)
    row_offsets = jnp.arange(block_length, dtype=jnp.int32)
    slot_ids = jnp.concatenate([local_ids, own_index[:, None]], 1)
    one_hot = slot_ids[..., None] == jnp.arange(window_blocks, dtype=jnp.int32)
    flat_width = block_length * head_dim
    win_pairs = jnp.concatenate(
        [
            win_keys.reshape(window_blocks, flat_width),
            win_values.reshape(window_blocks, flat_width),
        ],
        1,
    )
    gathered = jnp.einsum(
        "bsw,wf->bsf", one_hot.astype(jnp.bfloat16), win_pairs, preferred_element_type=jnp.float32
    ).astype(jnp.bfloat16)
    key_matrix_rows = gathered[..., :flat_width].reshape(
        blocks_dev, (SEL + 1) * block_length, head_dim
    )
    value_matrix_rows = gathered[..., flat_width:].reshape(
        blocks_dev, (SEL + 1) * block_length, head_dim
    )
    mask_sel = jnp.broadcast_to(
        live_slots[:, None, :, None], (blocks_dev, block_length, SEL, block_length)
    )
    causal = row_offsets[None, :] <= row_offsets[:, None]
    mask_own = jnp.broadcast_to(
        causal[None, :, None, :], (blocks_dev, block_length, 1, block_length)
    )
    permitted_mask = jnp.concatenate([mask_sel, mask_own], 2).reshape(
        blocks_dev, block_length, (SEL + 1) * block_length
    )
    query_blocks, key_part, value_part = tile_grads(
        query_tile_set,
        gradient_tiles,
        sum_tiles,
        key_matrix_rows,
        value_matrix_rows,
        permitted_mask,
        scaling,
    )
    parts = jnp.concatenate(
        [
            key_part.reshape(blocks_dev, SEL + 1, flat_width),
            value_part.reshape(blocks_dev, SEL + 1, flat_width),
        ],
        2,
    )
    win_grads = jnp.einsum(
        "bsw,bsf->wf", one_hot.astype(jnp.float32), parts, precision=lax.Precision.HIGHEST
    )
    key_pieces = win_grads[:, :flat_width].reshape(REACH + 1, tok_rows, head_dim)
    value_pieces = win_grads[:, flat_width:].reshape(REACH + 1, tok_rows, head_dim)
    query_grad = query_blocks.reshape(tok_rows, group_size * head_dim).astype(jnp.bfloat16)
    key_total = key_pieces[REACH]
    value_total = value_pieces[REACH]
    for offset in range(1, REACH + 1):
        back_key, back_value = passed_along(
            (key_pieces[REACH - offset], value_pieces[REACH - offset]), "kv", -offset
        )
        key_total = key_total + back_key
        value_total = value_total + back_value
    key_grad = key_total.astype(jnp.bfloat16)
    value_grad = value_total.astype(jnp.bfloat16)
    whole_inputs = lax.all_gather(inputs, "tp", axis=1, tiled=True)
    weight_grad = lax.psum_scatter(
        lax.dot_general(
            whole_inputs, value_grad, (((0,), (0,)), ((), ())), preferred_element_type=jnp.float32
        ),
        "kv",
        scatter_dimension=0,
        tiled=True,
    )
    return (query_grad, key_grad, value_grad, weight_grad)


def solution(mesh):
    in_specs = (
        P("kv", "tp"),
        P("kv", "tp"),
        P("kv", "tp"),
        P("tp", "kv"),
        P("kv", "tp"),
        P("kv", "tp", None),
        P("kv", "tp"),
    )
    out_specs = (P("kv", "tp"), P("kv", "tp"), P("kv", "tp"), P("kv", "tp"))
    return jax.shard_map(shards, mesh=mesh, in_specs=in_specs, out_specs=out_specs, check_vma=False)
```

profile of v0, /device:TPU:0, one launch (start us, length us, event | category | flops | bytes accessed | tf_op | source)
XLA Modules:
  0.0 144.5 jit_solution(9270566848137589164)
XLA Ops:
  7.2 5.1 %collective-permute-start = (bf16[256,128]{1,0:T(8,128)(2,1)}, bf16[256,128]{1,0:T(8,128)(2,1)S(1)}, u32[]{:S(2)}, u32[]{:S(2)}) collective-permute-start(bf16[256,128]{1,0:T(8,128)(2,1)} %param.8), channel_id=1, source_target_pairs={{0,8},{2,10},{4,12},{6,14},{8,16},{10,18},{12,20},{14,22},{16,24},... | collective-permute-start | bytes 196616 | tf_op jit(solution)/shard_map/ppermute | solution.py:13
  12.3 2.6 %collective-permute-start.1 = (bf16[256,128]{1,0:T(8,128)(2,1)}, bf16[256,128]{1,0:T(8,128)(2,1)S(1)}, u32[]{:S(2)}, u32[]{:S(2)}) collective-permute-start(bf16[256,128]{1,0:T(8,128)(2,1)} %param.8), channel_id=1, source_target_pairs={{0,6},{2,8},{4,10},{6,12},{8,14},{10,16},{12,18},{14,20},{16,22},{... | collective-permute-start | bytes 196616 | tf_op jit(solution)/shard_map/ppermute | solution.py:13
  14.9 3.4 %collective-permute-start.2 = (bf16[256,128]{1,0:T(8,128)(2,1)}, bf16[256,128]{1,0:T(8,128)(2,1)S(1)}, u32[]{:S(2)}, u32[]{:S(2)}) collective-permute-start(bf16[256,128]{1,0:T(8,128)(2,1)} %param.8), channel_id=1, source_target_pairs={{0,4},{2,6},{4,8},{6,10},{8,12},{10,14},{12,16},{14,18},{16,20},{1... | collective-permute-start | bytes 196616 | tf_op jit(solution)/shard_map/ppermute | solution.py:13
  18.4 2.6 %collective-permute-start.3 = (bf16[256,128]{1,0:T(8,128)(2,1)}, bf16[256,128]{1,0:T(8,128)(2,1)S(1)}, u32[]{:S(2)}, u32[]{:S(2)}) collective-permute-start(bf16[256,128]{1,0:T(8,128)(2,1)} %param.8), channel_id=1, source_target_pairs={{0,2},{2,4},{4,6},{6,8},{8,10},{10,12},{12,14},{14,16},{16,18},{18... | collective-permute-start | bytes 196616 | tf_op jit(solution)/shard_map/ppermute | solution.py:13
  21.0 3.5 %collective-permute-start.4 = (bf16[256,128]{1,0:T(8,128)(2,1)}, bf16[256,128]{1,0:T(8,128)(2,1)S(1)}, u32[]{:S(2)}, u32[]{:S(2)}) collective-permute-start(bf16[256,128]{1,0:T(8,128)(2,1)} %param.9), channel_id=1, source_target_pairs={{0,8},{2,10},{4,12},{6,14},{8,16},{10,18},{12,20},{14,22},{16,24},... | collective-permute-start | bytes 196616 | tf_op jit(solution)/shard_map/ppermute | solution.py:13
  24.6 1.5 %reshape.113 = bf16[4,64,6,128]{3,2,1,0:T(8,128)(2,1)S(1)} reshape(bf16[256,768]{1,0:T(8,128)(2,1)} %param.11) | data formatting | bytes 786432 | tf_op jit(solution)/shard_map/reshape | solution.py:76
  26.1 0.7 broadcast_subtract_fusion
  26.8 0.8 broadcast_compare_fusion
  27.5 0.1 broadcast_in_dim.14
  27.7 0.2 pad_add_fusion
  27.9 0.4 copy.25
  28.3 1.3 reshape.110
  29.6 0.1 reshape.111
  29.8 3.0 %collective-permute-start.5 = (bf16[256,128]{1,0:T(8,128)(2,1)S(1)}, bf16[256,128]{1,0:T(8,128)(2,1)S(1)}, u32[]{:S(2)}, u32[]{:S(2)}) collective-permute-start(bf16[256,128]{1,0:T(8,128)(2,1)S(1)} %copy-done.6), channel_id=1, source_target_pairs={{0,6},{2,8},{4,10},{6,12},{8,14},{10,16},{12,18},{14,20},{16,22},{... | collective-permute-start | bytes 196616 | tf_op jit(solution)/shard_map/ppermute | solution.py:13
  32.8 2.8 %collective-permute-start.6 = (bf16[256,128]{1,0:T(8,128)(2,1)S(1)}, bf16[256,128]{1,0:T(8,128)(2,1)S(1)}, u32[]{:S(2)}, u32[]{:S(2)}) collective-permute-start(bf16[256,128]{1,0:T(8,128)(2,1)S(1)} %copy-done.6), channel_id=1, source_target_pairs={{0,4},{2,6},{4,8},{6,10},{8,12},{10,14},{12,16},{14,18},{16,20},{1... | collective-permute-start | bytes 196616 | tf_op jit(solution)/shard_map/ppermute | solution.py:13
  35.6 1.3 collective-permute-start.7
  37.0 0.2 reshape.107
  37.3 0.2 collective-permute-done.6
  37.5 0.3 collective-permute-done.7
  37.8 0.2 reshape.108
  38.0 0.8 convolution_convert_fusion
  38.8 0.1 fusion.30
  38.9 1.2 reshape.118
  40.1 0.3 reshape.117
  40.5 1.8 %fusion.18 = f32[4,576,64,6]{1,2,3,0:T(8,128)S(1)} fusion(bf16[4,576,128,1]{2,1,0,3:T(8,128)(2,1)} %reshape.118, bf16[4,64,6,128]{3,2,1,0:T(8,128)(2,1)S(1)} %reshape.113), kind=kOutput, calls=%fused_computation.26 | convolution fusion | flops 226492416 | bytes 4521984 | tf_op jit(solution)/shard_map/nevu,npu->nvep/dot_general | solution.py:32
  42.3 1.8 %fusion.3 = (f32[4,6,64]{2,1,0:T(8,128)S(1)}, f32[4,6,64,576]{3,2,1,0:T(8,128)S(1)}) fusion(f32[4,576,64,6]{1,2,3,0:T(8,128)S(1)} %fusion.18, f32[4,6,64]{2,1,0:T(8,128)S(1)} %bitcast.60, bf16[4,64,6,128]{3,2,1,0:T(8,128)(2,1)S(1)} %copy-done.2, bf16[4,576,128,1]{2,1,0,3:T(8,128)(2,1)S(1)} %reshape.117, pred[4,64,576]{2,1,0:T(8,128)(4,1)S(1)} %copy.25), kind=kOutput, calls=%fused_computation.7 | convolution fusion | flops 230914560 | bytes 8220672 | tf_op jit(solution)/shard_map/nevu,npu->nvep/dot_general | solution.py:26
  44.1 1.8 %fusion.10 = f32[4,576,128]{2,1,0:T(8,128)} fusion(f32[4,6,64,576]{3,2,1,0:T(8,128)S(1)} %get-tuple-element.29, bf16[4,64,6,128]{3,2,1,0:T(8,128)(2,1)S(1)} %reshape.113), kind=kOutput, calls=%fused_computation.16 | convolution fusion | flops 227377152 | bytes 5111808 | tf_op jit(solution)/shard_map/cxie,cixa->cea/dot_general | solution.py:50
  45.9 0.5 fusion.5
  46.4 1.3 copy-done
  47.7 1.8 %fusion.13 = f32[4,576,128]{2,1,0:T(8,128)} fusion(bf16[4,6,64,576]{3,2,1,0:T(8,128)(2,1)S(1)} %fusion.5, bf16[4,64,6,128]{3,2,1,0:T(8,128)(2,1)S(1)} %copy-done.2), kind=kOutput, calls=%fused_computation.18 | convolution fusion | flops 226787328 | bytes 3342336 | tf_op jit(solution)/shard_map/cxie,cixa->cea/dot_general | solution.py:45
  49.5 1.4 reshape.114
  51.0 2.7 %reshape.115 = f32[4,9,8192]{2,1,0:T(8,128)} reshape(f32[4,576,128]{2,1,0:T(8,128)} %fusion.10) | data formatting | bytes 2359296 | tf_op jit(solution)/shard_map/reshape | solution.py:120
  53.6 3.4 %convolution_bitcast_fusion = f32[20,16384]{1,0:T(8,128)S(1)} fusion(f32[4,9,8192]{2,1,0:T(8,128)} %reshape.115, f32[4,9,8192]{2,1,0:T(8,128)S(1)} %reshape.114, s32[4,9]{1,0:T(4,128)S(1)} %pad_add_fusion.1), kind=kOutput, calls=%fused_computation.1 | convolution fusion | flops 142148304 | bytes 3670160 | tf_op jit(solution)/shard_map/bsw,bsf->wf/dot_general | solution.py:124
  57.0 0.2 fusion.31
  57.2 0.1 squeeze.40
  57.3 1.3 collective-permute-start.12
  58.6 0.1 squeeze.41
  58.7 1.3 collective-permute-start.13
  60.0 0.1 squeeze.42
  60.1 1.3 collective-permute-start.14
  61.4 0.1 squeeze.43
  61.5 1.5 %collective-permute-start.15 = (f32[256,128]{1,0:T(8,128)S(1)}, f32[256,128]{1,0:T(8,128)S(1)}, u32[]{:S(2)}, u32[]{:S(2)}) collective-permute-start(f32[256,128]{1,0:T(8,128)S(1)} %squeeze.43), channel_id=1, source_target_pairs={{8,0},{10,2},{12,4},{14,6},{16,8},{18,10},{20,12},{22,14},{24,16},... | collective-permute-start | bytes 393224 | tf_op jit(solution)/shard_map/ppermute | solution.py:13
  63.0 0.1 squeeze.39
  63.1 6.7 %collective-permute-done.13 = f32[256,128]{1,0:T(8,128)S(1)} collective-permute-done((f32[256,128]{1,0:T(8,128)S(1)}, f32[256,128]{1,0:T(8,128)S(1)}, u32[]{:S(2)}, u32[]{:S(2)}) %collective-permute-start.13) | collective-permute-done | bytes 131104 | tf_op jit(solution)/shard_map/ppermute | solution.py:13
  69.9 1.2 collective-permute-done.14
  71.1 5.4 %collective-permute-done.15 = f32[256,128]{1,0:T(8,128)S(1)} collective-permute-done((f32[256,128]{1,0:T(8,128)S(1)}, f32[256,128]{1,0:T(8,128)S(1)}, u32[]{:S(2)}, u32[]{:S(2)}) %collective-permute-start.15) | collective-permute-done | bytes 131104 | tf_op jit(solution)/shard_map/ppermute | solution.py:13
  76.5 1.8 %convolution_bitcast_fusion.1 = f32[3072,128]{0,1:T(8,128)S(1)} fusion(bf16[256,128]{1,0:T(8,128)(2,1)S(1)} %add_convert_fusion, bf16[256,3072]{1,0:T(8,128)(2,1)} %all-gather.2.cloned.1.call-done), kind=kOutput, calls=%fused_computation.13 | convolution fusion | flops 201326592 | bytes 3211264 | tf_op jit(solution)/shard_map/dot_general | solution.py:142
  78.3 1.7 %copy.37 = f32[3072,128]{1,0:T(8,128)} copy(f32[3072,128]{0,1:T(8,128)S(1)} %convolution_bitcast_fusion.1) | data formatting | bytes 3145728
  80.0 0.1 squeeze.37
  80.1 1.4 collective-permute-start.10
  81.6 0.1 squeeze.38
  81.7 1.3 collective-permute-start.11
  83.0 0.1 squeeze.35
  83.1 1.3 collective-permute-start.8
  84.4 0.7 squeeze.36
  85.1 1.3 collective-permute-start.9
  86.4 0.6 fusion.15
  87.1 0.1 squeeze.34
  87.2 0.3 copy.29
  87.4 0.8 copy.52
  88.2 1.0 collective-permute-done.11
  89.3 3.7 %collective-permute-done.9 = f32[256,128]{1,0:T(8,128)} collective-permute-done((f32[256,128]{1,0:T(8,128)}, f32[256,128]{1,0:T(8,128)}, u32[]{:S(2)}, u32[]{:S(2)}) %collective-permute-start.9) | collective-permute-done | bytes 131104 | tf_op jit(solution)/shard_map/ppermute | solution.py:13
  93.0 1.8 %add_convert_fusion.1 = bf16[256,128]{1,0:T(8,128)(2,1)} fusion(f32[256,128]{1,0:T(8,128)} %collective-permute-done.11, f32[256,128]{1,0:T(8,128)} %collective-permute-done.10, f32[256,128]{1,0:T(8,128)} %collective-permute-done.9, f32[256,128]{1,0:T(8,128)S(1)} %squeeze.34, f32[256,128]{1,0:T(8,128)} %collective-permute-done.8), kind=kLoop, calls=%fused_computation.36 | loop fusion | flops 163840 | bytes 720896 | tf_op jit(solution)/shard_map/convert_element_type | solution.py:138
  94.8 42.9 %reduce-scatter.4.cloned.1.call-done = f32[192,128]{1,0:T(8,128)} async-done(((f32[3072,128]{1,0:T(8,128)}), f32[192,128]{1,0:T(8,128)}) %reduce-scatter.4.cloned.1.call-update) | async-done | bytes 98320
  (46 shorter events, 0.5 us)
Async XLA Ops:
  7.2 22.6 %copy-start.6 = (bf16[256,128]{1,0:T(8,128)(2,1)S(1)}, bf16[256,128]{1,0:T(8,128)(2,1)}, u32[]{:S(2)}) copy-start(bf16[256,128]{1,0:T(8,128)(2,1)} %param.9) | copy-start | bytes 196612
  7.2 21.1 %copy-start.3 = (bf16[256,768]{1,0:T(8,128)(2,1)S(1)}, bf16[256,768]{1,0:T(8,128)(2,1)}, u32[]{:S(2)}) copy-start(bf16[256,768]{1,0:T(8,128)(2,1)} %param.7) | copy-start | bytes 1179652
  7.2 22.4 %copy-start.7 = (f32[6,256]{1,0:T(8,128)S(1)}, f32[6,256]{1,0:T(8,128)}, u32[]{:S(2)}) copy-start(f32[6,256]{1,0:T(8,128)} %param.10) | copy-start | bytes 18436
  7.2 69.3 %all-gather.2.cloned.1.call-start = ((), (), s32[]{:S(2)}) async-start(), calls=%async_computation.1 | async-start | bytes 2359296 | tf_op jit(solution)/shard_map/all_gather | solution.py:140
  7.2 22.5 %collective-permute-start = (bf16[256,128]{1,0:T(8,128)(2,1)}, bf16[256,128]{1,0:T(8,128)(2,1)S(1)}, u32[]{:S(2)}, u32[]{:S(2)}) collective-permute-start(bf16[256,128]{1,0:T(8,128)(2,1)} %param.8), channel_id=1, source_target_pairs={{0,8},{2,10},{4,12},{6,14},{8,16},{10,18},{12,20},{14,22},{16,24},... | collective-permute-start | bytes 196616 | tf_op jit(solution)/shard_map/ppermute | solution.py:13
  12.3 20.4 %collective-permute-start.1 = (bf16[256,128]{1,0:T(8,128)(2,1)}, bf16[256,128]{1,0:T(8,128)(2,1)S(1)}, u32[]{:S(2)}, u32[]{:S(2)}) collective-permute-start(bf16[256,128]{1,0:T(8,128)(2,1)} %param.8), channel_id=1, source_target_pairs={{0,6},{2,8},{4,10},{6,12},{8,14},{10,16},{12,18},{14,20},{16,22},{... | collective-permute-start | bytes 196616 | tf_op jit(solution)/shard_map/ppermute | solution.py:13
  14.9 20.7 %collective-permute-start.2 = (bf16[256,128]{1,0:T(8,128)(2,1)}, bf16[256,128]{1,0:T(8,128)(2,1)S(1)}, u32[]{:S(2)}, u32[]{:S(2)}) collective-permute-start(bf16[256,128]{1,0:T(8,128)(2,1)} %param.8), channel_id=1, source_target_pairs={{0,4},{2,6},{4,8},{6,10},{8,12},{10,14},{12,16},{14,18},{16,20},{1... | collective-permute-start | bytes 196616 | tf_op jit(solution)/shard_map/ppermute | solution.py:13
  18.4 18.6 %collective-permute-start.3 = (bf16[256,128]{1,0:T(8,128)(2,1)}, bf16[256,128]{1,0:T(8,128)(2,1)S(1)}, u32[]{:S(2)}, u32[]{:S(2)}) collective-permute-start(bf16[256,128]{1,0:T(8,128)(2,1)} %param.8), channel_id=1, source_target_pairs={{0,2},{2,4},{4,6},{6,8},{8,10},{10,12},{12,14},{14,16},{16,18},{18... | collective-permute-start | bytes 196616 | tf_op jit(solution)/shard_map/ppermute | solution.py:13
  21.0 16.2 %collective-permute-start.4 = (bf16[256,128]{1,0:T(8,128)(2,1)}, bf16[256,128]{1,0:T(8,128)(2,1)S(1)}, u32[]{:S(2)}, u32[]{:S(2)}) collective-permute-start(bf16[256,128]{1,0:T(8,128)(2,1)} %param.9), channel_id=1, source_target_pairs={{0,8},{2,10},{4,12},{6,14},{8,16},{10,18},{12,20},{14,22},{16,24},... | collective-permute-start | bytes 196616 | tf_op jit(solution)/shard_map/ppermute | solution.py:13
  24.5 12.4 %copy-start.5 = (bf16[256,128]{1,0:T(8,128)(2,1)S(1)}, bf16[256,128]{1,0:T(8,128)(2,1)}, u32[]{:S(2)}) copy-start(bf16[256,128]{1,0:T(8,128)(2,1)} %param.8) | copy-start | bytes 196612
  24.5 113.1 %reduce-scatter.4.cloned.1.call-start = ((), (), s32[]{:S(2)}) async-start(), calls=%async_computation.2 | async-start | bytes 1671168
  29.8 7.5 %collective-permute-start.5 = (bf16[256,128]{1,0:T(8,128)(2,1)S(1)}, bf16[256,128]{1,0:T(8,128)(2,1)S(1)}, u32[]{:S(2)}, u32[]{:S(2)}) collective-permute-start(bf16[256,128]{1,0:T(8,128)(2,1)S(1)} %copy-done.6), channel_id=1, source_target_pairs={{0,6},{2,8},{4,10},{6,12},{8,14},{10,16},{12,18},{14,20},{16,22},{... | collective-permute-start | bytes 196616 | tf_op jit(solution)/shard_map/ppermute | solution.py:13
  32.8 4.7 %collective-permute-start.6 = (bf16[256,128]{1,0:T(8,128)(2,1)S(1)}, bf16[256,128]{1,0:T(8,128)(2,1)S(1)}, u32[]{:S(2)}, u32[]{:S(2)}) collective-permute-start(bf16[256,128]{1,0:T(8,128)(2,1)S(1)} %copy-done.6), channel_id=1, source_target_pairs={{0,4},{2,6},{4,8},{6,10},{8,12},{10,14},{12,16},{14,18},{16,20},{1... | collective-permute-start | bytes 196616 | tf_op jit(solution)/shard_map/ppermute | solution.py:13
  35.6 2.2 %collective-permute-start.7 = (bf16[256,128]{1,0:T(8,128)(2,1)S(1)}, bf16[256,128]{1,0:T(8,128)(2,1)S(1)}, u32[]{:S(2)}, u32[]{:S(2)}) collective-permute-start(bf16[256,128]{1,0:T(8,128)(2,1)S(1)} %copy-done.6), channel_id=1, source_target_pairs={{0,2},{2,4},{4,6},{6,8},{8,10},{10,12},{12,14},{14,16},{16,18},{18... | collective-permute-start | bytes 196616 | tf_op jit(solution)/shard_map/ppermute | solution.py:13
  40.5 1.8 %copy-start.2 = (bf16[4,64,6,128]{3,2,1,0:T(8,128)(2,1)S(1)}, bf16[4,64,6,128]{3,2,1,0:T(8,128)(2,1)}, u32[]{:S(2)}) copy-start(bf16[4,64,6,128]{3,2,1,0:T(8,128)(2,1)} %reshape.110) | copy-start | bytes 1179652
  46.4 1.3 copy-start
  57.3 5.8 %collective-permute-start.12 = (f32[256,128]{1,0:T(8,128)S(1)}, f32[256,128]{1,0:T(8,128)S(1)}, u32[]{:S(2)}, u32[]{:S(2)}) collective-permute-start(f32[256,128]{1,0:T(8,128)S(1)} %squeeze.40), channel_id=1, source_target_pairs={{2,0},{4,2},{6,4},{8,6},{10,8},{12,10},{14,12},{16,14},{18,16},{20... | collective-permute-start | bytes 393224 | tf_op jit(solution)/shard_map/ppermute | solution.py:13
  58.7 11.1 %collective-permute-start.13 = (f32[256,128]{1,0:T(8,128)S(1)}, f32[256,128]{1,0:T(8,128)S(1)}, u32[]{:S(2)}, u32[]{:S(2)}) collective-permute-start(f32[256,128]{1,0:T(8,128)S(1)} %squeeze.41), channel_id=1, source_target_pairs={{4,0},{6,2},{8,4},{10,6},{12,8},{14,10},{16,12},{18,14},{20,16},{2... | collective-permute-start | bytes 393224 | tf_op jit(solution)/shard_map/ppermute | solution.py:13
  60.1 11.0 %collective-permute-start.14 = (f32[256,128]{1,0:T(8,128)S(1)}, f32[256,128]{1,0:T(8,128)S(1)}, u32[]{:S(2)}, u32[]{:S(2)}) collective-permute-start(f32[256,128]{1,0:T(8,128)S(1)} %squeeze.42), channel_id=1, source_target_pairs={{6,0},{8,2},{10,4},{12,6},{14,8},{16,10},{18,12},{20,14},{22,16},{... | collective-permute-start | bytes 393224 | tf_op jit(solution)/shard_map/ppermute | solution.py:13
  61.5 14.9 %collective-permute-start.15 = (f32[256,128]{1,0:T(8,128)S(1)}, f32[256,128]{1,0:T(8,128)S(1)}, u32[]{:S(2)}, u32[]{:S(2)}) collective-permute-start(f32[256,128]{1,0:T(8,128)S(1)} %squeeze.43), channel_id=1, source_target_pairs={{8,0},{10,2},{12,4},{14,6},{16,8},{18,10},{20,12},{22,14},{24,16},... | collective-permute-start | bytes 393224 | tf_op jit(solution)/shard_map/ppermute | solution.py:13
  76.5 3.5 %copy-start.4 = (bf16[256,128]{1,0:T(8,128)(2,1)}, bf16[256,128]{1,0:T(8,128)(2,1)S(1)}, u32[]{:S(2)}) copy-start(bf16[256,128]{1,0:T(8,128)(2,1)S(1)} %add_convert_fusion) | copy-start | bytes 196612
  80.0 6.4 %copy-start.1 = (bf16[4,6,64,576]{3,2,1,0:T(8,128)(2,1)S(1)}, bf16[4,6,64,576]{3,2,1,0:T(8,128)(2,1)}, u32[]{:S(2)}) copy-start(bf16[4,6,64,576]{3,2,1,0:T(8,128)(2,1)} %copy-done) | copy-start | bytes 5308420
  80.1 8.1 %collective-permute-start.10 = (f32[256,128]{1,0:T(8,128)S(1)}, f32[256,128]{1,0:T(8,128)}, u32[]{:S(2)}, u32[]{:S(2)}) collective-permute-start(f32[256,128]{1,0:T(8,128)S(1)} %squeeze.37), channel_id=1, source_target_pairs={{6,0},{8,2},{10,4},{12,6},{14,8},{16,10},{18,12},{20,14},{22,16},{... | collective-permute-start | bytes 393224 | tf_op jit(solution)/shard_map/ppermute | solution.py:13
  81.7 7.6 %collective-permute-start.11 = (f32[256,128]{1,0:T(8,128)S(1)}, f32[256,128]{1,0:T(8,128)}, u32[]{:S(2)}, u32[]{:S(2)}) collective-permute-start(f32[256,128]{1,0:T(8,128)S(1)} %squeeze.38), channel_id=1, source_target_pairs={{8,0},{10,2},{12,4},{14,6},{16,8},{18,10},{20,12},{22,14},{24,16},... | collective-permute-start | bytes 393224 | tf_op jit(solution)/shard_map/ppermute | solution.py:13
  83.1 6.2 %collective-permute-start.8 = (f32[256,128]{1,0:T(8,128)S(1)}, f32[256,128]{1,0:T(8,128)}, u32[]{:S(2)}, u32[]{:S(2)}) collective-permute-start(f32[256,128]{1,0:T(8,128)S(1)} %squeeze.35), channel_id=1, source_target_pairs={{2,0},{4,2},{6,4},{8,6},{10,8},{12,10},{14,12},{16,14},{18,16},{20... | collective-permute-start | bytes 393224 | tf_op jit(solution)/shard_map/ppermute | solution.py:13
  85.1 7.9 %collective-permute-start.9 = (f32[256,128]{1,0:T(8,128)}, f32[256,128]{1,0:T(8,128)}, u32[]{:S(2)}, u32[]{:S(2)}) collective-permute-start(f32[256,128]{1,0:T(8,128)} %squeeze.36), channel_id=1, source_target_pairs={{4,0},{6,2},{8,4},{10,6},{12,8},{14,10},{16,12},{18,14},{20,16},{2... | collective-permute-start | bytes 393224 | tf_op jit(solution)/shard_map/ppermute | solution.py:13
Sparse Core Ops, SparseCore 0:
  24.7 25.0 all-gather.1
  80.1 57.4 reduce-scatter.3
where the time goes:
time: 145 us
  waiting for transfers between devices  61.6 us (42%)
  starting transfers between devices  35 us (24%)
  local copies, waits for them, and re-layouts  15.5 us (11%)
  between operations  14.6 us (10%)
  matrix products  13.8 us (10%)
  other arithmetic  4 us (3%)
    unnamed x3, waiting for transfers between devices  42.9 us
    ppermute x16, starting transfers between devices, passed_along(): lax.ppermute(value, axis, [(source, source + steps) for source in range(l...  34.9 us
    ppermute x16, waiting for transfers between devices, passed_along(): lax.ppermute(value, axis, [(source, source + steps) for source in range(l...  18.6 us
    unnamed x26, local copies, waits for them, and re-layouts  3.85 us
    dot_general x1, matrix products, shards(): jnp.einsum('bsw,bsf->wf', one_hot.astype(jnp.float32), parts, precision=l...  3.36 us
  transfers between devices with their start and end apart: 18, of which 8 were waited for; matrix products, arithmetic and copies ran while one was open for 20% of the time, Pallas kernels for 0%

commit v1 on v0

v1 whole, which is shorter than its diff:
```python
import functools

import jax
import jax.numpy as jnp
from jax import lax
from jax.experimental import pallas as pl
from jax.experimental.pallas import tpu as pltpu
from jax.sharding import PartitionSpec as P

REACH = 4
MASKED = -1e30
LOG2E = 1.4426950408889634
MESH = pl.DeviceIdType.MESH
NT = (((1,), (1,)), ((), ()))


def kernel(
    nk,
    nt,
    bias_ref,
    lse_ref,
    k_ref,
    v_ref,
    q_hbm,
    do_hbm,
    x_hbm,
    qg_ref,
    kg_ref,
    vg_ref,
    wg_ref,
    q_s,
    do_s,
    x_s,
    q6,
    do6,
    kw,
    vw,
    kt,
    own_bias,
    p_s,
    pb_s,
    ds_s,
    dvo,
    dvi,
    dko,
    dki,
    dv_own,
    x_t,
    x_in,
    vpair,
    po,
    ri,
    ld_sem,
    k_send,
    k_recv,
    v_send,
    v_recv,
    dv_send,
    dv_recv,
    dk_send,
    dk_recv,
    x_send,
    x_recv,
    x_loc,
    vp_send,
    vp_recv,
    rs_send,
    rs_recv,
):
    me = lax.axis_index("kv")
    tp = lax.axis_index("tp")
    core = lax.rem(me, 2)
    chip = me // 2
    sib = me + 1 - 2 * core
    chips = nk // 2
    tok, hd = k_ref.shape
    heads = lse_ref.shape[0]
    nblk = bias_ref.shape[1]
    blk = tok // nblk
    scale = hd**-0.5
    per_tp, _, rw, _ = x_t.shape

    loads = [
        pltpu.make_async_copy(src, dst, ld_sem.at[i])
        for i, (src, dst) in enumerate(((x_hbm, x_s), (q_hbm, q_s), (do_hbm, do_s)))
    ]
    for load in loads:
        load.start()

    barrier = pltpu.get_barrier_semaphore()

    @pl.loop(1, nk)
    def _(j):
        pl.semaphore_signal(
            barrier, inc=1, device_id=(lax.rem(me + j, nk), tp), device_id_type=MESH
        )

    for dt in range(1, nt):
        for kv in (me, sib):
            pl.semaphore_signal(
                barrier, inc=1, device_id=(kv, lax.rem(tp + dt, nt)), device_id_type=MESH
            )
    pl.semaphore_wait(barrier, nk - 1 + 2 * (nt - 1))

    def remote(src, dst, send, recv, kv, t=None):
        return pltpu.make_async_remote_copy(
            src_ref=src,
            dst_ref=dst,
            send_sem=send,
            recv_sem=recv,
            device_id=(kv, tp if t is None else t),
            device_id_type=MESH,
        )

    def k_copy(o):
        return remote(k_ref, kw.at[o], k_send.at[o], k_recv.at[o], me + o)

    def v_copy(o):
        return remote(v_ref, vw.at[o], v_send.at[o], v_recv.at[o], me + o)

    def dv_copy(o):
        return remote(dvo.at[o], dvi.at[o], dv_send.at[o], dv_recv.at[o], me - o)

    def dk_copy(o):
        return remote(dko.at[o], dki.at[o], dk_send.at[o], dk_recv.at[o], me - o)

    for copy in (k_copy, v_copy):
        for o in range(1, REACH + 1):

            @pl.when(me + o < nk)
            def _():
                copy(o).start()

    loads[0].wait()
    x_t[...] = x_s[...].T.reshape(x_t.shape)
    x_copies = [
        remote(x_t.at[:, 1 - core], x_in.at[tp, core], x_send.at[0, 1], x_recv.at[tp, core], sib)
    ]
    for dt in range(1, nt):
        other = lax.rem(tp + dt, nt)
        for s, kv, par in ((0, me, core), (1, sib, 1 - core)):
            x_copies.append(
                remote(
                    x_t.at[:, par],
                    x_in.at[tp, core],
                    x_send.at[dt, s],
                    x_recv.at[tp, core],
                    kv,
                    other,
                )
            )
    for copy in x_copies:
        copy.start()
    x_local = pltpu.make_async_copy(x_t.at[:, core], x_in.at[tp, core], x_loc)
    x_local.start()

    zero = jnp.zeros((tok, hd), jnp.bfloat16)
    for o in range(1, REACH + 1):

        @pl.when(me < o)
        def _():
            kw[o] = zero
            vw[o] = zero

        @pl.when(me + o >= nk)
        def _():
            dvi[o] = zero
            dki[o] = zero

    kw[0] = k_ref[...]
    vw[0] = v_ref[...]
    loads[1].wait()
    loads[2].wait()
    for a in range(heads):
        q6[a] = q_s[:, a * hd : (a + 1) * hd]
        do6[a] = do_s[:, a * hd : (a + 1) * hd]
    key_row = lax.broadcasted_iota(jnp.int32, (blk, tok), 0)
    pos = lax.broadcasted_iota(jnp.int32, (blk, tok), 1)
    for j in range(nblk):
        own_bias[j * blk : (j + 1) * blk, :] = jnp.where(
            key_row + j * blk > pos, MASKED, bias_ref[0, j : j + 1, :]
        )

    def first(o, own):
        keys = kw[o]
        for a in range(heads):
            s = lax.dot_general(keys, q6[a], NT, preferred_element_type=jnp.float32)
            s = s * (scale * LOG2E)
            lse = lse_ref[a : a + 1, :] * LOG2E
            if own:
                p = jnp.exp2(s + (own_bias[...] - lse))
            else:
                rows = bias_ref[o] - lse
                p = jnp.exp2(s.reshape(nblk, blk, tok) + rows[:, None, :]).reshape(tok, tok)
            p_s[a, o] = p
            pb_s[:, a * tok : (a + 1) * tok] = p.astype(jnp.bfloat16)
        return jnp.dot(
            pb_s[...], do6[...].reshape(heads * tok, hd), preferred_element_type=jnp.float32
        )

    dv_own[...] = first(0, True)

    @pl.loop(1, REACH + 1)
    def _(o):
        @pl.when(me >= o)
        def _():
            k_copy(o).wait_recv()

        dvo[o] = first(o, False).astype(jnp.bfloat16)

        @pl.when(me >= o)
        def _():
            dv_copy(o).start()

    kt[...] = kw[...].reshape((REACH + 1) * tok, hd).T
    for o in range(1, REACH + 1):

        @pl.when(me >= o)
        def _():
            v_copy(o).wait_recv()

    for a in range(heads):
        gw = lax.dot_general(
            vw[...].reshape((REACH + 1) * tok, hd), do6[a], NT, preferred_element_type=jnp.float32
        )
        p = p_s[a].reshape((REACH + 1) * tok, tok)
        delta = jnp.sum(p * gw, 0, keepdims=True)
        ds = (p * (gw - delta)).astype(jnp.bfloat16)
        ds_s[:, a * tok : (a + 1) * tok] = ds
        dq_t = jnp.dot(kt[...], ds, preferred_element_type=jnp.float32) * scale
        qg_ref[:, a * hd : (a + 1) * hd] = dq_t.T.astype(jnp.bfloat16)

    value = dv_own[...]
    for o in range(1, REACH + 1):

        @pl.when(me + o < nk)
        def _():
            dv_copy(o).wait_recv()

        value = value + dvi[o].astype(jnp.float32)
    value = value.astype(jnp.bfloat16)
    vg_ref[...] = value
    vpair[pl.ds(core, 1)] = value[None]
    pair = remote(vpair.at[core], vpair.at[core], vp_send, vp_recv, sib)
    pair.start()

    dk = (
        jnp.dot(ds_s[...], q6[...].reshape(heads * tok, hd), preferred_element_type=jnp.float32)
        * scale
    )
    dko[...] = dk.astype(jnp.bfloat16).reshape(REACH + 1, tok, hd)

    x_local.wait()
    for t in range(nt):
        for c in range(2):

            @pl.when((t != tp) | (c != core))
            def _():
                remote(
                    x_t.at[:, 0], x_in.at[t, c], x_send.at[0, 1], x_recv.at[t, c], sib
                ).wait_recv()

    remote(
        vpair.at[core], vpair.at[1 - core], vp_send, vp_recv, sib
    ).wait_recv()
    for t in range(nt):
        part = jnp.dot(
            x_in[t, 0].reshape(per_tp * rw, tok), vpair[0], preferred_element_type=jnp.float32
        ) + jnp.dot(
            x_in[t, 1].reshape(per_tp * rw, tok), vpair[1], preferred_element_type=jnp.float32
        )
        po[t * per_tp : (t + 1) * per_tp] = part.astype(jnp.bfloat16).reshape(per_tp, rw, hd)

    def rs_copy(j):
        to = lax.rem(chip + j, chips)
        return remote(po.at[to], ri.at[chip], rs_send.at[j], rs_recv.at[chip], to * 2 + core)

    @pl.loop(1, chips)
    def _(j):
        rs_copy(j).start()

    for o in range(1, REACH + 1):

        @pl.when(me >= o)
        def _():
            dk_copy(o).start()

    ri[pl.ds(chip, 1)] = po[pl.ds(chip, 1)]
    key = dk[:tok]
    for o in range(1, REACH + 1):

        @pl.when(me + o < nk)
        def _():
            dk_copy(o).wait_recv()

        key = key + dki[o].astype(jnp.float32)
    kg_ref[...] = key.astype(jnp.bfloat16)

    @pl.loop(1, chips)
    def _(j):
        src = lax.rem(chip + j, chips)
        remote(po.at[src], ri.at[src], rs_send.at[j], rs_recv.at[src], src * 2 + core).wait_recv()

    wg_ref[...] = jnp.sum(ri[...].astype(jnp.float32), 0)

    for o in range(1, REACH + 1):

        @pl.when(me + o < nk)
        def _():
            k_copy(o).wait_send()
            v_copy(o).wait_send()

        @pl.when(me >= o)
        def _():
            dv_copy(o).wait_send()
            dk_copy(o).wait_send()

    for copy in x_copies:
        copy.wait_send()
    pair.wait_send()

    @pl.loop(1, chips)
    def _(j):
        rs_copy(j).wait_send()


def shards(nk, nt, queries, keys, values, log_sums, out_grad, chosen, inputs):
    tok, hd = keys.shape
    heads = queries.shape[1] // hd
    nblk = chosen.shape[0]
    blk = tok // nblk
    feats = inputs.shape[1]
    rw = feats * nt // nk
    per_tp = feats // (2 * rw)
    span = REACH + 1
    device = lax.axis_index("kv")
    listed = chosen[:, 0, :]
    own_ids = device * nblk + jnp.arange(nblk, dtype=jnp.int32)
    win_ids = (
        (device - jnp.arange(span, dtype=jnp.int32)[:, None]) * nblk
        + jnp.arange(nblk, dtype=jnp.int32)[None, :]
    ).reshape(span * nblk)
    hit = (listed[None] == win_ids[:, None, None]) & (listed < own_ids[:, None])[None]
    allowed = jnp.any(hit, 2) | (win_ids[:, None] == own_ids[None, :])
    bias = jnp.repeat(jnp.where(allowed, 0.0, MASKED).astype(jnp.float32), blk, axis=1)
    bias = bias.reshape(span, nblk, tok)

    bf, f32 = jnp.bfloat16, jnp.float32
    dma = pltpu.SemaphoreType.DMA
    vmem = pl.BlockSpec(memory_space=pltpu.VMEM)
    hbm = pl.BlockSpec(memory_space=pl.ANY)
    return pl.pallas_call(
        functools.partial(kernel, nk, nt),
        out_shape=(
            jax.ShapeDtypeStruct((tok, heads * hd), bf),
            jax.ShapeDtypeStruct((tok, hd), bf),
            jax.ShapeDtypeStruct((tok, hd), bf),
            jax.ShapeDtypeStruct((rw, hd), f32),
        ),
        in_specs=[vmem, vmem, vmem, vmem, hbm, hbm, hbm],
        out_specs=(vmem, vmem, vmem, vmem),
        scratch_shapes=[
            pltpu.VMEM((tok, heads * hd), bf),
            pltpu.VMEM((tok, heads * hd), bf),
            pltpu.VMEM((tok, feats), bf),
            pltpu.VMEM((heads, tok, hd), bf),
            pltpu.VMEM((heads, tok, hd), bf),
            pltpu.VMEM((span, tok, hd), bf),
            pltpu.VMEM((span, tok, hd), bf),
            pltpu.VMEM((hd, span * tok), bf),
            pltpu.VMEM((tok, tok), f32),
            pltpu.VMEM((heads, span, tok, tok), f32),
            pltpu.VMEM((tok, heads * tok), bf),
            pltpu.VMEM((span * tok, heads * tok), bf),
            pltpu.VMEM((span, tok, hd), bf),
            pltpu.VMEM((span, tok, hd), bf),
            pltpu.VMEM((span, tok, hd), bf),
            pltpu.VMEM((span, tok, hd), bf),
            pltpu.VMEM((tok, hd), f32),
            pltpu.VMEM((per_tp, 2, rw, tok), bf),
            pltpu.VMEM((nt, 2, per_tp, rw, tok), bf),
            pltpu.VMEM((2, tok, hd), bf),
            pltpu.VMEM((nk // 2, rw, hd), bf),
            pltpu.VMEM((nk // 2, rw, hd), bf),
            dma((3,)),
            dma((span,)),
            dma((span,)),
            dma((span,)),
            dma((span,)),
            dma((span,)),
            dma((span,)),
            dma((span,)),
            dma((span,)),
            dma((nt, 2)),
            dma((nt, 2)),
            dma,
            dma,
            dma,
            dma((nk // 2,)),
            dma((nk // 2,)),
        ],
        compiler_params=pltpu.CompilerParams(
            collective_id=0, has_side_effects=True, vmem_limit_bytes=60 * 1024 * 1024
        ),
    )(bias, log_sums, keys, values, queries, out_grad, inputs)


def solution(mesh):
    in_specs = (
        P("kv", "tp"),
        P("kv", "tp"),
        P("kv", "tp"),
        P("tp", "kv"),
        P("kv", "tp"),
        P("kv", "tp", None),
        P("kv", "tp"),
    )
    out_specs = (P("kv", "tp"), P("kv", "tp"), P("kv", "tp"), P("kv", "tp"))
    return jax.shard_map(
        functools.partial(shards, mesh.shape["kv"], mesh.shape["tp"]),
        mesh=mesh,
        in_specs=in_specs,
        out_specs=out_specs,
        check_vma=False,
    )
```

time: 145 us -> 48.8 us (0.34)
  waiting for transfers between devices: 61.6 us -> 0 us
  Pallas kernels: 0 us -> 41.7 us
  starting transfers between devices: 35 us -> 0 us
  between operations: 14.6 us -> 0.69 us
  matrix products: 13.8 us -> 0 us
  local copies, waits for them, and re-layouts: 15.5 us -> 5.84 us
  other arithmetic: 4 us -> 0.32 us
    unnamed x3 -> x0, waiting for transfers between devices: 42.9 us -> none
    pallas_call x0 -> x1, Pallas kernels: none -> 41.7 us  [shards(): pl.pallas_call(functools.partial(kernel, nk, nt), out_shape=(jax.ShapeDty...]
    ppermute x16 -> x0, starting transfers between devices: 34.9 us -> none  [passed_along(): lax.ppermute(value, axis, [(source, source + steps) for source in range(l...]
    ppermute x16 -> x0, waiting for transfers between devices: 18.6 us -> none  [passed_along(): lax.ppermute(value, axis, [(source, source + steps) for source in range(l...]
    dot_general x8 -> x0, matrix products: 13.8 us -> none  [the longest x1 3.36 us: shards(): jnp.einsum('bsw,bsf->wf', one_hot.astype(jnp.float32), parts, precision=l...]
    reshape x10 -> x0, local copies, waits for them, and re-layouts: 8.82 us -> none  [the longest x1 2.67 us: shards(): value_part.reshape(blocks_dev, SEL + 1, flat_width)]
    convert_element_type x3 -> x0, other arithmetic: 2.31 us -> none  [the longest x1 1.78 us: shards(): key_grad = key_total.astype(jnp.bfloat16)]
    squeeze x10 -> x0, local copies, waits for them, and re-layouts: 1.57 us -> none  [the longest x4 1.02 us: shards(): key_pieces[REACH - offset]]
  transfers between devices with their start and end apart: 18 -> 0, of which waited for: 8 -> 0; matrix products, arithmetic and copies ran while one was open for 20% -> 0% of each run, Pallas kernels for 0% -> 0%
where the time goes in v1:
time: 48.8 us; the launch traced here: 48.5 us
  Pallas kernels  41.7 us (85%)
  local copies, waits for them, and re-layouts  5.84 us (12%)
  between operations  0.69 us (1%)
    pallas_call x1, Pallas kernels, shards(): pl.pallas_call(functools.partial(kernel, nk, nt), out_shape=(jax.ShapeDty...  41.7 us
    unnamed x12, local copies, waits for them, and re-layouts  4.88 us

profile of v1, /device:TPU:0, one launch (start us, length us, event | category | flops | bytes accessed | tf_op | source)
XLA Modules:
  0.0 48.5 jit_solution(11247595037233290520)
XLA Ops:
  0.6 0.0 copy-start.3
  0.7 0.7 %copy-done.3 = s32[4,1,8]{2,1,0:T(1,128)S(1)} copy-done((s32[4,1,8]{2,1,0:T(1,128)S(1)}, s32[4,1,8]{2,1,0:T(1,128)}, u32[]{:S(2)}) %copy-start.3) | copy-done | bytes 152
  1.3 0.1 broadcast_compare_fusion
  1.4 0.1 iota_add_fusion
  1.5 0.1 add.41
  1.6 0.1 and_reduce_fusion
  1.6 0.1 or_select_fusion
  1.7 0.1 copy.11
  1.8 0.1 broadcast_in_dim.18
  1.9 0.7 %reshape_reshape.3.bias_ref = f32[5,4,256]{2,1,0:T(4,128)} reshape(f32[20,4,64]{2,1,0:T(4,128)S(1)} %broadcast_in_dim.18) | data formatting | bytes 40960 | tf_op jit(solution)/shard_map/reshape;reshape | solution.py:346
  2.6 41.7 %shard_map.102 = (bf16[256,768]{1,0:T(8,128)(2,1)}, bf16[256,128]{1,0:T(8,128)(2,1)}, bf16[256,128]{1,0:T(8,128)(2,1)}, f32[192,128]{1,0:T(8,128)}) custom-call(f32[5,4,256]{2,1,0:T(4,128)} %reshape_reshape.3.bias_ref, f32[6,256]{1,0:T(8,128)} %lse_ref.1, bf16[256,128]{1,0:T(8,128)(2,1)} %k_ref.1, bf16[256,128]{1,0:T(8,128)(2,1)} %v_ref.1, ...), custom_call_target="tpu_custom_call" | custom-call | tf_op jit(solution)/shard_map/pallas_call | solution.py:352
  44.3 0.0 copy-start.2
  44.3 1.8 %copy.16 = bf16[256,768]{1,0:T(8,128)(2,1)} copy(bf16[256,768]{1,0:T(8,128)(2,1)} %get-tuple-element.8) | data formatting | bytes 786432
  46.1 0.0 copy-done.2
  46.1 0.0 copy-start.1
  46.1 0.6 %copy.17 = bf16[256,128]{1,0:T(8,128)(2,1)} copy(bf16[256,128]{1,0:T(8,128)(2,1)S(1)} %copy-done.2) | data formatting | bytes 131072
  46.7 0.2 copy-done.1
  47.0 0.0 copy-start
  47.0 0.6 %copy.18 = bf16[256,128]{1,0:T(8,128)(2,1)} copy(bf16[256,128]{1,0:T(8,128)(2,1)S(1)} %copy-done.1) | data formatting | bytes 131072
  47.6 0.3 copy-done
  47.9 0.6 %copy.19 = f32[192,128]{1,0:T(8,128)} copy(f32[192,128]{1,0:T(8,128)S(1)} %copy-done) | data formatting | bytes 196608
  (2 shorter events, 0.0 us)
Async XLA Ops:
  0.6 0.7 %copy-start.3 = (s32[4,1,8]{2,1,0:T(1,128)S(1)}, s32[4,1,8]{2,1,0:T(1,128)}, u32[]{:S(2)}) copy-start(s32[4,1,8]{2,1,0:T(1,128)} %param.12) | copy-start | bytes 388
  44.3 1.8 %copy-start.2 = (bf16[256,128]{1,0:T(8,128)(2,1)S(1)}, bf16[256,128]{1,0:T(8,128)(2,1)}, u32[]{:S(2)}) copy-start(bf16[256,128]{1,0:T(8,128)(2,1)} %get-tuple-element.9) | copy-start | bytes 196612
  46.1 0.9 %copy-start.1 = (bf16[256,128]{1,0:T(8,128)(2,1)S(1)}, bf16[256,128]{1,0:T(8,128)(2,1)}, u32[]{:S(2)}) copy-start(bf16[256,128]{1,0:T(8,128)(2,1)} %get-tuple-element.10) | copy-start | bytes 196612
  47.0 0.9 %copy-start = (f32[192,128]{1,0:T(8,128)S(1)}, f32[192,128]{1,0:T(8,128)}, u32[]{:S(2)}) copy-start(f32[192,128]{1,0:T(8,128)} %get-tuple-element.11) | copy-start | bytes 294916

commit v2 on v1

--- a/solution.py
+++ b/solution.py
@@ -17,7 +17,7 @@
 def kernel(
     nk,
     nt,
-    bias_ref,
+    chosen_ref,
     lse_ref,
     k_ref,
     v_ref,
@@ -36,6 +36,7 @@
     kw,
     vw,
     kt,
+    bias_ref,
     own_bias,
     p_s,
     pb_s,
@@ -75,7 +76,7 @@
     chips = nk // 2
     tok, hd = k_ref.shape
     heads = lse_ref.shape[0]
-    nblk = bias_ref.shape[1]
+    nblk = chosen_ref.shape[0]
     blk = tok // nblk
     scale = hd**-0.5
     per_tp, _, rw, _ = x_t.shape
@@ -133,22 +134,32 @@
 
     loads[0].wait()
     x_t[...] = x_s[...].T.reshape(x_t.shape)
-    x_copies = [
-        remote(x_t.at[:, 1 - core], x_in.at[tp, core], x_send.at[0, 1], x_recv.at[tp, core], sib)
-    ]
-    for dt in range(1, nt):
-        other = lax.rem(tp + dt, nt)
-        for s, kv, par in ((0, me, core), (1, sib, 1 - core)):
-            x_copies.append(
-                remote(
-                    x_t.at[:, par],
-                    x_in.at[tp, core],
-                    x_send.at[dt, s],
-                    x_recv.at[tp, core],
-                    kv,
-                    other,
+    half = per_tp // 2
+    x_copies = []
+    for h in range(2):
+        rows = pl.ds(h * half, half)
+        for dt in range(1, nt):
+            other = lax.rem(tp + dt, nt)
+            for s, kv, par in ((0, me, core), (1, sib, 1 - core)):
+                x_copies.append(
+                    remote(
+                        x_t.at[rows, par],
+                        x_in.at[tp, core, rows],
+                        x_send.at[h, dt, s],
+                        x_recv.at[h, tp, core],
+                        kv,
+                        other,
+                    )
                 )
+        x_copies.append(
+            remote(
+                x_t.at[rows, 1 - core],
+                x_in.at[tp, core, rows],
+                x_send.at[h, 0, 1],
+                x_recv.at[h, tp, core],
+                sib,
             )
+        )
     for copy in x_copies:
         copy.start()
     x_local = pltpu.make_async_copy(x_t.at[:, core], x_in.at[tp, core], x_loc)
@@ -174,6 +185,20 @@
     for a in range(heads):
         q6[a] = q_s[:, a * hd : (a + 1) * hd]
         do6[a] = do_s[:, a * hd : (a + 1) * hd]
+    row = lax.broadcasted_iota(jnp.int32, (nblk, tok), 0)
+    col = lax.broadcasted_iota(jnp.int32, (nblk, tok), 1)
+    marked = [jnp.full((nblk, tok), MASKED, jnp.float32) for _ in range(REACH + 1)]
+    for b in range(nblk):
+        in_block = (col >= b * blk) & (col < (b + 1) * blk)
+        marked[0] = jnp.where(in_block & (row == b), 0.0, marked[0])
+        for slot in range(chosen_ref.shape[2]):
+            block = chosen_ref[b, 0, slot]
+            block = jnp.where(block < me * nblk + b, block, -1)
+            for o in range(REACH + 1):
+                hit = in_block & (row + (me - o) * nblk == block)
+                marked[o] = jnp.where(hit & (block >= 0), 0.0, marked[o])
+    for o in range(REACH + 1):
+        bias_ref[o] = marked[o]
     key_row = lax.broadcasted_iota(jnp.int32, (blk, tok), 0)
     pos = lax.broadcasted_iota(jnp.int32, (blk, tok), 1)
     for j in range(nblk):
@@ -219,16 +244,54 @@
         def _():
             v_copy(o).wait_recv()
 
-    for a in range(heads):
+    def score_grad(a):
         gw = lax.dot_general(
             vw[...].reshape((REACH + 1) * tok, hd), do6[a], NT, preferred_element_type=jnp.float32
         )
         p = p_s[a].reshape((REACH + 1) * tok, tok)
         delta = jnp.sum(p * gw, 0, keepdims=True)
-        ds = (p * (gw - delta)).astype(jnp.bfloat16)
-        ds_s[:, a * tok : (a + 1) * tok] = ds
+        ds_s[:, a * tok : (a + 1) * tok] = (p * (gw - delta)).astype(jnp.bfloat16)
+
+    def query_part(a):
+        ds = ds_s[:, a * tok : (a + 1) * tok]
         dq_t = jnp.dot(kt[...], ds, preferred_element_type=jnp.float32) * scale
         qg_ref[:, a * hd : (a + 1) * hd] = dq_t.T.astype(jnp.bfloat16)
+
+    def rs_copy(to):
+        return remote(po.at[to], ri.at[chip], rs_send.at[to], rs_recv.at[chip], to * 2 + core)
+
+    def weight_part(dt, h):
+        t = lax.rem(tp + dt, nt)
+        rows = pl.ds(h * half, half)
+        for c in range(2):
+
+            @pl.when((t != tp) | (c != core))
+            def _():
+                remote(
+                    x_t.at[rows, 0],
+                    x_in.at[t, c, rows],
+                    x_send.at[0, 0, 1],
+                    x_recv.at[h, t, c],
+                    sib,
+                ).wait_recv()
+
+        part = jnp.dot(
+            x_in[t, 0, rows].reshape(half * rw, tok), vpair[0], preferred_element_type=jnp.float32
+        ) + jnp.dot(
+            x_in[t, 1, rows].reshape(half * rw, tok), vpair[1], preferred_element_type=jnp.float32
+        )
+        start = t * per_tp + h * half
+        po[pl.ds(start, half)] = part.astype(jnp.bfloat16).reshape(half, rw, hd)
+
+        @pl.loop(0, half)
+        def _(j):
+            @pl.when(start + j != chip)
+            def _():
+                rs_copy(start + j).start()
+
+    split = heads // 2
+    for a in range(split):
+        score_grad(a)
 
     value = dv_own[...]
     for o in range(1, REACH + 1):
@@ -243,50 +306,42 @@
     vpair[pl.ds(core, 1)] = value[None]
     pair = remote(vpair.at[core], vpair.at[core], vp_send, vp_recv, sib)
     pair.start()
-
-    dk = (
-        jnp.dot(ds_s[...], q6[...].reshape(heads * tok, hd), preferred_element_type=jnp.float32)
-        * scale
-    )
-    dko[...] = dk.astype(jnp.bfloat16).reshape(REACH + 1, tok, hd)
-
+    score_grad(split)
+    remote(vpair.at[core], vpair.at[1 - core], vp_send, vp_recv, sib).wait_recv()
     x_local.wait()
-    for t in range(nt):
-        for c in range(2):
-
-            @pl.when((t != tp) | (c != core))
+    for dt in range(1, nt):
+        weight_part(dt, 0)
+    for h in range(2):
+        weight_part(0, h)
+    for a in range(split + 1, heads):
+        score_grad(a)
+
+    for o in range(REACH, -1, -1):
+        dk = (
+            jnp.dot(
+                ds_s[o * tok : (o + 1) * tok, :],
+                q6[...].reshape(heads * tok, hd),
+                preferred_element_type=jnp.float32,
+            )
+            * scale
+        )
+        if o == 0:
+            key = dk
+        else:
+            dko[o] = dk.astype(jnp.bfloat16)
+
+            @pl.when(me >= o)
             def _():
-                remote(
-                    x_t.at[:, 0], x_in.at[t, c], x_send.at[0, 1], x_recv.at[t, c], sib
-                ).wait_recv()
-
-    remote(
-        vpair.at[core], vpair.at[1 - core], vp_send, vp_recv, sib
-    ).wait_recv()
-    for t in range(nt):
-        part = jnp.dot(
-            x_in[t, 0].reshape(per_tp * rw, tok), vpair[0], preferred_element_type=jnp.float32
-        ) + jnp.dot(
-            x_in[t, 1].reshape(per_tp * rw, tok), vpair[1], preferred_element_type=jnp.float32
-        )
-        po[t * per_tp : (t + 1) * per_tp] = part.astype(jnp.bfloat16).reshape(per_tp, rw, hd)
-
-    def rs_copy(j):
-        to = lax.rem(chip + j, chips)
-        return remote(po.at[to], ri.at[chip], rs_send.at[j], rs_recv.at[chip], to * 2 + core)
-
-    @pl.loop(1, chips)
-    def _(j):
-        rs_copy(j).start()
-
-    for o in range(1, REACH + 1):
-
-        @pl.when(me >= o)
-        def _():
-            dk_copy(o).start()
+                dk_copy(o).start()
+
+    for a in range(split):
+        query_part(a)
+    for dt in range(1, nt):
+        weight_part(dt, 1)
+    for a in range(split, heads):
+        query_part(a)
 
     ri[pl.ds(chip, 1)] = po[pl.ds(chip, 1)]
-    key = dk[:tok]
     for o in range(1, REACH + 1):
 
         @pl.when(me + o < nk)
@@ -299,7 +354,7 @@
     @pl.loop(1, chips)
     def _(j):
         src = lax.rem(chip + j, chips)
-        remote(po.at[src], ri.at[src], rs_send.at[j], rs_recv.at[src], src * 2 + core).wait_recv()
+        remote(po.at[src], ri.at[src], rs_send.at[src], rs_recv.at[src], src * 2 + core).wait_recv()
 
     wg_ref[...] = jnp.sum(ri[...].astype(jnp.float32), 0)
 
@@ -321,35 +376,34 @@
 
     @pl.loop(1, chips)
     def _(j):
-        rs_copy(j).wait_send()
+        rs_copy(lax.rem(chip + j, chips)).wait_send()
+
+
+def finish(*refs):
+    count = len(refs) // 2
+    sems = refs[-1]
+    copies = [
+        pltpu.make_async_copy(refs[i], refs[count + i], sems.at[i]) for i in range(count)
+    ]
+    for copy in copies:
+        copy.start()
+    for copy in copies:
+        copy.wait()
 
 
 def shards(nk, nt, queries, keys, values, log_sums, out_grad, chosen, inputs):
     tok, hd = keys.shape
     heads = queries.shape[1] // hd
     nblk = chosen.shape[0]
-    blk = tok // nblk
     feats = inputs.shape[1]
     rw = feats * nt // nk
     per_tp = feats // (2 * rw)
     span = REACH + 1
-    device = lax.axis_index("kv")
-    listed = chosen[:, 0, :]
-    own_ids = device * nblk + jnp.arange(nblk, dtype=jnp.int32)
-    win_ids = (
-        (device - jnp.arange(span, dtype=jnp.int32)[:, None]) * nblk
-        + jnp.arange(nblk, dtype=jnp.int32)[None, :]
-    ).reshape(span * nblk)
-    hit = (listed[None] == win_ids[:, None, None]) & (listed < own_ids[:, None])[None]
-    allowed = jnp.any(hit, 2) | (win_ids[:, None] == own_ids[None, :])
-    bias = jnp.repeat(jnp.where(allowed, 0.0, MASKED).astype(jnp.float32), blk, axis=1)
-    bias = bias.reshape(span, nblk, tok)
-
     bf, f32 = jnp.bfloat16, jnp.float32
     dma = pltpu.SemaphoreType.DMA
     vmem = pl.BlockSpec(memory_space=pltpu.VMEM)
     hbm = pl.BlockSpec(memory_space=pl.ANY)
-    return pl.pallas_call(
+    parts = pl.pallas_call(
         functools.partial(kernel, nk, nt),
         out_shape=(
             jax.ShapeDtypeStruct((tok, heads * hd), bf),
@@ -357,7 +411,7 @@
             jax.ShapeDtypeStruct((tok, hd), bf),
             jax.ShapeDtypeStruct((rw, hd), f32),
         ),
-        in_specs=[vmem, vmem, vmem, vmem, hbm, hbm, hbm],
+        in_specs=[pl.BlockSpec(memory_space=pltpu.SMEM), vmem, vmem, vmem, hbm, hbm, hbm],
         out_specs=(vmem, vmem, vmem, vmem),
         scratch_shapes=[
             pltpu.VMEM((tok, heads * hd), bf),
@@ -368,6 +422,7 @@
             pltpu.VMEM((span, tok, hd), bf),
             pltpu.VMEM((span, tok, hd), bf),
             pltpu.VMEM((hd, span * tok), bf),
+            pltpu.VMEM((span, nblk, tok), f32),
             pltpu.VMEM((tok, tok), f32),
             pltpu.VMEM((heads, span, tok, tok), f32),
             pltpu.VMEM((tok, heads * tok), bf),
@@ -391,8 +446,8 @@
             dma((span,)),
             dma((span,)),
             dma((span,)),
-            dma((nt, 2)),
-            dma((nt, 2)),
+            dma((2, nt, 2)),
+            dma((2, nt, 2)),
             dma,
             dma,
             dma,
@@ -402,7 +457,14 @@
         compiler_params=pltpu.CompilerParams(
             collective_id=0, has_side_effects=True, vmem_limit_bytes=60 * 1024 * 1024
         ),
-    )(bias, log_sums, keys, values, queries, out_grad, inputs)
+    )(chosen, log_sums, keys, values, queries, out_grad, inputs)
+    return pl.pallas_call(
+        finish,
+        out_shape=tuple(jax.ShapeDtypeStruct(part.shape, part.dtype) for part in parts),
+        in_specs=[vmem] * len(parts),
+        out_specs=(hbm,) * len(parts),
+        scratch_shapes=[dma((len(parts),))],
+    )(*parts)
 
 
 def solution(mesh):

time: 48.8 us -> 37.7 us (0.77)
  the two profiles are of different devices: /device:TPU:0 before, /device:TPU:13 now
where the time goes in v2:
time: 37.7 us; the launch traced here: 37.5 us
  Pallas kernels  36.8 us (98%)
  between operations  0.64 us (2%)
    pallas_call x1, Pallas kernels, shards(): pl.pallas_call(functools.partial(kernel, nk, nt), out_shape=(jax.ShapeDty...  34.9 us
    pallas_call x1, Pallas kernels, shards(): pl.pallas_call(finish, out_shape=tuple((jax.ShapeDtypeStruct(part.shape,...  1.93 us

profile of v2, /device:TPU:13, one launch (start us, length us, event | category | flops | bytes accessed | tf_op | source)
XLA Modules:
  0.0 37.5 jit_solution(12240225129630846908)
XLA Ops:
  0.6 34.9 %shard_map.102 = (bf16[256,768]{1,0:T(8,128)(2,1)}, bf16[256,128]{1,0:T(8,128)(2,1)}, bf16[256,128]{1,0:T(8,128)(2,1)}, f32[192,128]{1,0:T(8,128)}) custom-call(s32[4,1,8]{2,1,0:T(1,128)} %chosen_ref.1, f32[6,256]{1,0:T(8,128)} %lse_ref.1, bf16[256,128]{1,0:T(8,128)(2,1)} %k_ref.1, bf16[256,128]{1,0:T(8,128)(2,1)} %v_ref.1, bf16[256,768]{1,0:T(8,128)(2,1)} %q_hbm.1, ...), custom_call_target="tpu_custom_call" | custom-call | tf_op jit(solution)/shard_map/pallas_call | solution.py:406
  35.6 1.9 %shard_map.103 = (bf16[256,768]{1,0:T(8,128)(2,1)}, bf16[256,128]{1,0:T(8,128)(2,1)}, bf16[256,128]{1,0:T(8,128)(2,1)}, f32[192,128]{1,0:T(8,128)}) custom-call(bf16[256,768]{1,0:T(8,128)(2,1)} %get-tuple-element.8.refs_0_, bf16[256,128]{1,0:T(8,128)(2,1)} %get-tuple-element.9.refs_1_, bf16[256,128]{1,0:T(8,128)(2,1)} %get-tuple-element.10.refs_2_, ...), custom_call_target="tpu_custom_call" | custom-call | tf_op jit(solution)/shard_map/pallas_call | solution.py:461

commit v3 on v2

--- a/solution.py
+++ b/solution.py
@@ -45,13 +45,19 @@
     dvi,
     dko,
     dki,
-    dv_own,
+    dv_sum,
+    dk_sum,
+    dv_out,
+    dv_in,
+    dk_out,
+    dk_in,
     x_t,
     x_in,
     vpair,
     po,
     ri,
     ld_sem,
+    own_sem,
     k_send,
     k_recv,
     v_send,
@@ -125,8 +131,35 @@
     def dk_copy(o):
         return remote(dko.at[o], dki.at[o], dk_send.at[o], dk_recv.at[o], me - o)
 
+    def k_pass(u):
+        src = kw.at[2 * u + 2 * core]
+        return remote(src, kw.at[2 * u + 1], k_send.at[2 * u + 1], k_recv.at[2 * u + 1], sib)
+
+    def v_pass(u):
+        src = vw.at[2 * u + 2 * core]
+        return remote(src, vw.at[2 * u + 1], v_send.at[2 * u + 1], v_recv.at[2 * u + 1], sib)
+
+    def dv_hand(u):
+        return remote(
+            dv_out.at[u], dv_in.at[u], dv_send.at[2 * u + 1], dv_recv.at[2 * u + 1], sib
+        )
+
+    def dk_hand(u):
+        return remote(
+            dk_out.at[u], dk_in.at[u], dk_send.at[2 * u + 1], dk_recv.at[2 * u + 1], sib
+        )
+
+    def take_hands(hand, landed, sums):
+        for u in range(2):
+
+            @pl.when(me >= 2 * u + 2 * core)
+            def _():
+                hand(u).wait_recv()
+                slot = pl.ds(u + core, 1)
+                sums[slot] = sums[slot] + landed[u][None].astype(jnp.float32)
+
     for copy in (k_copy, v_copy):
-        for o in range(1, REACH + 1):
+        for o in (2, 4):
 
             @pl.when(me + o < nk)
             def _():
@@ -178,8 +211,20 @@
             dvi[o] = zero
             dki[o] = zero
 
-    kw[0] = k_ref[...]
-    vw[0] = v_ref[...]
+    own = [
+        pltpu.make_async_copy(src, dst.at[0], own_sem.at[n])
+        for n, (src, dst) in enumerate(((k_ref, kw), (v_ref, vw)))
+    ]
+    for copy in own:
+        copy.start()
+    for copy in own:
+        copy.wait()
+
+    @pl.when(core == 0)
+    def _():
+        k_pass(0).start()
+        v_pass(0).start()
+
     loads[1].wait()
     loads[2].wait()
     for a in range(heads):
@@ -223,26 +268,54 @@
             pb_s[...], do6[...].reshape(heads * tok, hd), preferred_element_type=jnp.float32
         )
 
-    dv_own[...] = first(0, True)
-
-    @pl.loop(1, REACH + 1)
-    def _(o):
+    dv_sum[0] = first(0, True)
+
+    @pl.loop(0, 2)
+    def _(u):
+        @pl.when(me >= 2 * u + 2)
+        def _():
+            k_copy(2 * u + 2).wait_recv()
+
+            @pl.when((u == 0) | (core == 1))
+            def _():
+                k_pass(jnp.where(u == 0, 1 - core, 1)).start()
+
+        dv_sum[u + 1] = first(2 * u + 2, False)
+
+        @pl.when(me >= 2 * u + 1)
+        def _():
+            k_pass(u).wait_recv()
+
+        dv_out[u] = first(2 * u + 1, False).astype(jnp.bfloat16)
+
+        @pl.when(me >= 2 * u + 1)
+        def _():
+            dv_hand(u).start()
+
+    for u in range(2):
+
+        @pl.when(me >= 2 * u + 2)
+        def _():
+            v_copy(2 * u + 2).wait_recv()
+
+            @pl.when((u == 0) | (core == 1))
+            def _():
+                v_pass(jnp.where(u == 0, 1 - core, 1)).start()
+
+    kt[...] = kw[...].reshape((REACH + 1) * tok, hd).T
+    take_hands(dv_hand, dv_in, dv_sum)
+    for o in (4, 2):
+        dvo[o] = dv_sum[o // 2].astype(jnp.bfloat16)
+
         @pl.when(me >= o)
         def _():
-            k_copy(o).wait_recv()
-
-        dvo[o] = first(o, False).astype(jnp.bfloat16)
-
-        @pl.when(me >= o)
-        def _():
             dv_copy(o).start()
 
-    kt[...] = kw[...].reshape((REACH + 1) * tok, hd).T
-    for o in range(1, REACH + 1):
-
-        @pl.when(me >= o)
-        def _():
-            v_copy(o).wait_recv()
+    for u in range(2):
+
+        @pl.when(me >= 2 * u + 1)
+        def _():
+            v_pass(u).wait_recv()
 
     def score_grad(a):
         gw = lax.dot_general(
@@ -293,8 +366,8 @@
     for a in range(split):
         score_grad(a)
 
-    value = dv_own[...]
-    for o in range(1, REACH + 1):
+    value = dv_sum[0]
+    for o in (2, 4):
 
         @pl.when(me + o < nk)
         def _():
@@ -309,14 +382,13 @@
     score_grad(split)
     remote(vpair.at[core], vpair.at[1 - core], vp_send, vp_recv, sib).wait_recv()
     x_local.wait()
-    for dt in range(1, nt):
-        weight_part(dt, 0)
     for h in range(2):
-        weight_part(0, h)
+        for dt in range(nt - 1, -1, -1):
+            weight_part(dt, h)
     for a in range(split + 1, heads):
         score_grad(a)
 
-    for o in range(REACH, -1, -1):
+    for o in (3, 1, 4, 2, 0):
         dk = (
             jnp.dot(
                 ds_s[o * tok : (o + 1) * tok, :],
@@ -325,24 +397,29 @@
             )
             * scale
         )
-        if o == 0:
-            key = dk
+        if o % 2 == 0:
+            dk_sum[o // 2] = dk
         else:
-            dko[o] = dk.astype(jnp.bfloat16)
+            dk_out[o // 2] = dk.astype(jnp.bfloat16)
 
             @pl.when(me >= o)
             def _():
-                dk_copy(o).start()
-
-    for a in range(split):
+                dk_hand(o // 2).start()
+
+    take_hands(dk_hand, dk_in, dk_sum)
+    for o in (4, 2):
+        dko[o] = dk_sum[o // 2].astype(jnp.bfloat16)
+
+        @pl.when(me >= o)
+        def _():
+            dk_copy(o).start()
+
+    for a in range(heads):
         query_part(a)
-    for dt in range(1, nt):
-        weight_part(dt, 1)
-    for a in range(split, heads):
-        query_part(a)
-
+
+    key = dk_sum[0]
     ri[pl.ds(chip, 1)] = po[pl.ds(chip, 1)]
-    for o in range(1, REACH + 1):
+    for o in (2, 4):
 
         @pl.when(me + o < nk)
         def _():
@@ -358,7 +435,7 @@
 
     wg_ref[...] = jnp.sum(ri[...].astype(jnp.float32), 0)
 
-    for o in range(1, REACH + 1):
+    for o in (2, 4):
 
         @pl.when(me + o < nk)
         def _():
@@ -369,6 +446,18 @@
         def _():
             dv_copy(o).wait_send()
             dk_copy(o).wait_send()
+
+    for u in range(2):
+
+        @pl.when(me >= 2 * u + 2 * core)
+        def _():
+            k_pass(u).wait_send()
+            v_pass(u).wait_send()
+
+        @pl.when(me >= 2 * u + 1)
+        def _():
+            dv_hand(u).wait_send()
+            dk_hand(u).wait_send()
 
     for copy in x_copies:
         copy.wait_send()
@@ -431,13 +520,19 @@
             pltpu.VMEM((span, tok, hd), bf),
             pltpu.VMEM((span, tok, hd), bf),
             pltpu.VMEM((span, tok, hd), bf),
-            pltpu.VMEM((tok, hd), f32),
+            pltpu.VMEM((3, tok, hd), f32),
+            pltpu.VMEM((3, tok, hd), f32),
+            pltpu.VMEM((2, tok, hd), bf),
+            pltpu.VMEM((2, tok, hd), bf),
+            pltpu.VMEM((2, tok, hd), bf),
+            pltpu.VMEM((2, tok, hd), bf),
             pltpu.VMEM((per_tp, 2, rw, tok), bf),
             pltpu.VMEM((nt, 2, per_tp, rw, tok), bf),
             pltpu.VMEM((2, tok, hd), bf),
             pltpu.VMEM((nk // 2, rw, hd), bf),
             pltpu.VMEM((nk // 2, rw, hd), bf),
             dma((3,)),
+            dma((2,)),
             dma((span,)),
             dma((span,)),
             dma((span,)),

time: 37.7 us -> 38.1 us (1.011)
  the two profiles are of different devices: /device:TPU:13 before, /device:TPU:0 now
where the time goes in v3:
time: 38.1 us; the launch traced here: 37.4 us
  Pallas kernels  36.7 us (96%)
  between operations  0.64 us (2%)
    pallas_call x1, Pallas kernels, shards(): pl.pallas_call(functools.partial(kernel, nk, nt), out_shape=(jax.ShapeDty...  34.8 us
    pallas_call x1, Pallas kernels, shards(): pl.pallas_call(finish, out_shape=tuple((jax.ShapeDtypeStruct(part.shape,...  1.93 us

profile of v3, /device:TPU:0, one launch (start us, length us, event | category | flops | bytes accessed | tf_op | source)
XLA Modules:
  0.0 37.4 jit_solution(11435511102674979779)
XLA Ops:
  0.6 34.8 %shard_map.102 = (bf16[256,768]{1,0:T(8,128)(2,1)}, bf16[256,128]{1,0:T(8,128)(2,1)}, bf16[256,128]{1,0:T(8,128)(2,1)}, f32[192,128]{1,0:T(8,128)}) custom-call(s32[4,1,8]{2,1,0:T(1,128)} %chosen_ref.1, f32[6,256]{1,0:T(8,128)} %lse_ref.1, bf16[256,128]{1,0:T(8,128)(2,1)} %k_ref.1, bf16[256,128]{1,0:T(8,128)(2,1)} %v_ref.1, bf16[256,768]{1,0:T(8,128)(2,1)} %q_hbm.1, ...), custom_call_target="tpu_custom_call" | custom-call | tf_op jit(solution)/shard_map/pallas_call | solution.py:495
  35.5 1.9 %shard_map.103 = (bf16[256,768]{1,0:T(8,128)(2,1)}, bf16[256,128]{1,0:T(8,128)(2,1)}, bf16[256,128]{1,0:T(8,128)(2,1)}, f32[192,128]{1,0:T(8,128)}) custom-call(bf16[256,768]{1,0:T(8,128)(2,1)} %get-tuple-element.8.refs_0_, bf16[256,128]{1,0:T(8,128)(2,1)} %get-tuple-element.9.refs_1_, bf16[256,128]{1,0:T(8,128)(2,1)} %get-tuple-element.10.refs_2_, ...), custom_call_target="tpu_custom_call" | custom-call | tf_op jit(solution)/shard_map/pallas_call | solution.py:556
